TPU v7x, 32 devices: a whole 2x2x4 slice. The times are simulated.
32 devices in a mesh: sp: 8 (over z, y), tp: 4 (over x, core).
Axes of the slice: x: 2, y: 2, z: 4, core: 2. Of those that a mesh axis runs over, the one named last changes fastest.
Arguments:
- stream: bfloat16 [2048, 2048], P('sp', 'tp'), may hold values from -6 to 6
- norm_gain: float32 [2, 2048], replicated, may hold values from 0.1 to 1.9
- w_value: bfloat16 [2, 2048, 1024], P(None, 'sp', 'tp'), may hold values from -0.125 to 0.125
- w_gate: bfloat16 [2, 2048, 1024], P(None, 'sp', 'tp'), may hold values from -0.125 to 0.125
- conv_taps: float32 [2, 128, 1024], P(None, None, 'tp'), as said below
- channel_gain: float32 [2, 1024], P(None, 'tp'), may hold values from 0.1 to 1.9
- w_out: bfloat16 [2, 1024, 2048], P(None, 'tp', 'sp'), may hold values from -0.1875 to 0.1875
Outputs:
- result: bfloat16 [2048, 2048], P('sp', 'tp')
Inputs may be any that keep to these rules, and one draw needn't show every extreme that they name: `conv_taps`: taps of each block of 128 consecutive channels share a scale factor of its own.
All inputs are finite; a program needn't handle non-finite values.
Results may differ from a plain program's by a relative error of at most 0.012.
Values may be sent and summed in bfloat16 or wider, within the bound.
A program may use at most 64 MiB of HBM per device.

v0:
```python
import jax
import jax.numpy as jnp
from jax import lax
from jax.sharding import PartitionSpec as P

C = 1024
LAYERS = 2


def from_behind(value, axis, steps):
    count = lax.axis_size(axis)
    initial, last = (max(0, -steps), min(count, count - steps))
    return lax.ppermute(value, axis, [(source, source + steps) for source in range(initial, last)])


def shards(stream, norm_gain, w_value, w_gate, conv_taps, channel_gain, w_out):
    x = stream
    tokens_here = stream.shape[0]
    local_ch = w_value.shape[2]
    taps = conv_taps.shape[1]
    for layer in range(LAYERS):
        whole = lax.all_gather(x, "tp", axis=1, tiled=True).astype(jnp.float32)
        normed = (
            whole
            * lax.rsqrt(jnp.mean(whole * whole, axis=1, keepdims=True) + 1e-06)
            * norm_gain[layer]
        ).astype(jnp.bfloat16)
        value_whole, gate_whole = (
            lax.all_gather(w_value[layer], "sp", axis=0, tiled=True),
            lax.all_gather(w_gate[layer], "sp", axis=0, tiled=True),
        )
        value = jnp.dot(normed, value_whole, preferred_element_type=jnp.float32)
        gate = jnp.dot(normed, gate_whole, preferred_element_type=jnp.float32)
        glu = (value * jax.nn.sigmoid(gate)).astype(jnp.bfloat16)
        before = from_behind(glu[tokens_here - taps :], "sp", 1)
        padded = jnp.concatenate([before[1:], glu], axis=0).astype(jnp.float32)
        conv = lax.conv_general_dilated(
            padded[None],
            conv_taps[layer][:, None, :],
            (1,),
            "VALID",
            dimension_numbers=("NWC", "WIO", "NWC"),
            feature_group_count=local_ch,
            precision=lax.Precision.HIGHEST,
        )[0]
        mean = lax.psum(jnp.sum(conv, axis=1, keepdims=True), "tp") / C
        centred = conv - mean
        spread = lax.psum(jnp.sum(centred * centred, axis=1, keepdims=True), "tp") / C
        act = jax.nn.silu(centred * lax.rsqrt(spread + 1e-05) * channel_gain[layer]).astype(
            jnp.bfloat16
        )
        out_whole = lax.all_gather(w_out[layer], "sp", axis=1, tiled=True)
        terms = jnp.dot(act, out_whole, preferred_element_type=jnp.float32)
        branch = lax.psum_scatter(terms, "tp", scatter_dimension=1, tiled=True)
        x = (x.astype(jnp.float32) + branch).astype(jnp.bfloat16)
    return x


def solution(mesh):
    return jax.shard_map(
        shards,
        mesh=mesh,
        in_specs=(
            P("sp", "tp"),
            P(),
            P(None, "sp", "tp"),
            P(None, "sp", "tp"),
            P(None, None, "tp"),
            P(None, "tp"),
            P(None, "tp", "sp"),
        ),
        out_specs=P("sp", "tp"),
        check_vma=False,
    )
```

profile of v0, /device:TPU:0, one launch (start us, length us, event | category | flops | bytes accessed | tf_op | source)
XLA Modules:
  0.0 370.0 jit_solution(6867189528916284857)
XLA Ops:
  6.5 0.0 copy-start.5
  6.5 0.0 all-gather.15.cloned.1.call-start
  6.5 0.7 all-gather.15.cloned.1.call-update
  7.3 0.0 all-gather.19.cloned.1.call-start
  7.3 1.7 fusion.46
  9.0 0.0 all-gather.19.cloned.1.call-update
  9.0 0.0 all-gather.21.cloned.1.call-start
  9.1 1.7 fusion.45
  10.8 0.0 all-gather.21.cloned.1.call-update
  10.8 0.0 all-gather.23.cloned.1.call-start
  10.8 1.7 fusion.47
  12.5 0.0 all-gather.23.cloned.1.call-update
  12.6 0.0 reduce-scatter.3.cloned.1.call-start
  12.6 0.0 copy-done.5
  12.6 0.0 copy-done.4
  12.7 15.7 %all-gather.15.cloned.1.call-done = bf16[256,2048]{1,0:T(8,128)(2,1)} async-done(((bf16[256,512]{1,0:T(8,128)(2,1)}), bf16[256,2048]{1,0:T(8,128)(2,1)}) %all-gather.15.cloned.1.call-update) | async-done | bytes 1048592 | tf_op jit(solution)/shard_map/all_gather | solution.py:22
  28.4 1.6 fusion
  30.0 40.8 %all-gather.19.cloned.1.call-done = bf16[1,2048,256]{2,1,0:T(8,128)(2,1)} async-done(((bf16[1,256,256]{2,1,0:T(8,128)(2,1)}), bf16[1,2048,256]{2,1,0:T(8,128)(2,1)}) %all-gather.19.cloned.1.call-update) | async-done | bytes 1048592 | tf_op jit(solution)/shard_map/all_gather | solution.py:29
  70.8 2.0 fusion.24
  72.8 0.0 copy-start.6
  72.8 39.1 %all-gather.21.cloned.1.call-done = bf16[1,2048,256]{2,1,0:T(8,128)(2,1)} async-done(((bf16[1,256,256]{2,1,0:T(8,128)(2,1)}), bf16[1,2048,256]{2,1,0:T(8,128)(2,1)}) %all-gather.21.cloned.1.call-update) | async-done | bytes 1048592 | tf_op jit(solution)/shard_map/all_gather | solution.py:30
  111.9 0.0 copy-done.1
  111.9 1.7 fusion.14
  113.7 2.5 collective-permute-start
  116.2 0.0 copy-done.6
  116.2 1.9 collective-permute-done
  118.1 4.8 %fusion.50 = (f32[256]{0:T(256)S(1)}, f32[1,256,256]{2,0,1:T(1,128)S(1)}) fusion(f32[1,128,256]{2,1,0:T(8,128)S(1)} %get-tuple-element.6, bf16[1,383,256]{2,1,0:T(8,128)(2,1)S(1)} %maximum_bitcast_fusion), kind=kOutput, calls=%fused_computation.70 | convolution fusion | flops 100728576 | bytes 590336 | tf_op jit(solution)/shard_map/conv_general_dilated | solution.py:37
  123.0 5.7 %psum.28 = f32[256,1]{0,1:T(1,128)S(1)} all-reduce(f32[256,1]{0,1:T(1,128)S(1)} %bitcast.72), channel_id=1, replica_groups=mesh['sp'=8,'tp'=4] {'tp'}, use_global_device_ids=true, to_apply=%region_2.0 | all-reduce | flops 256 | bytes 2048 | tf_op jit(solution)/shard_map/psum | solution.py:46
  128.6 0.2 multiply_reduce_fusion.1
  128.8 7.0 %psum.29 = f32[256,1]{0,1:T(1,128)S(1)} all-reduce(f32[256,1]{0,1:T(1,128)S(1)} %bitcast.68), channel_id=1, replica_groups=mesh['sp'=8,'tp'=4] {'tp'}, use_global_device_ids=true, to_apply=%region_4.0 | all-reduce | flops 256 | bytes 2048 | tf_op jit(solution)/shard_map/psum | solution.py:48
  135.8 16.2 %all-gather.23.cloned.1.call-done = bf16[1,256,2048]{2,1,0:T(8,128)(2,1)} async-done(((bf16[1,256,256]{2,1,0:T(8,128)(2,1)}), bf16[1,256,2048]{2,1,0:T(8,128)(2,1)}) %all-gather.23.cloned.1.call-update) | async-done | bytes 1048592 | tf_op jit(solution)/shard_map/all_gather | solution.py:52
  152.0 3.1 fusion.21
  155.1 0.0 reduce-scatter.3.cloned.1.call-update
  155.1 0.0 all-gather.17.cloned.1.call-start
  155.2 30.3 %reduce-scatter.3.cloned.1.call-done = f32[256,512]{1,0:T(8,128)} async-done(((f32[256,2048]{1,0:T(8,128)}), f32[256,512]{1,0:T(8,128)}) %reduce-scatter.3.cloned.1.call-update) | async-done | bytes 524304 | tf_op jit(solution)/shard_map/reduce_scatter | solution.py:54
  185.4 0.0 copy-done.3
  185.4 1.8 add_convert_fusion.1
  187.3 0.0 all-gather.17.cloned.1.call-update
  187.3 0.0 all-gather.25.cloned.1.call-start
  187.3 0.7 all-gather.25.cloned.1.call-update
  188.0 0.0 all-gather.27.cloned.1.call-start
  188.1 0.7 all-gather.27.cloned.1.call-update
  188.8 0.0 all-gather.29.cloned.1.call-start
  188.8 0.7 all-gather.29.cloned.1.call-update
  189.5 0.0 reduce-scatter.5.cloned.1.call-start
  189.6 14.6 %all-gather.17.cloned.1.call-done = bf16[256,2048]{1,0:T(8,128)(2,1)} async-done(((bf16[256,512]{1,0:T(8,128)(2,1)}), bf16[256,2048]{1,0:T(8,128)(2,1)}) %all-gather.17.cloned.1.call-update) | async-done | bytes 1048592 | tf_op jit(solution)/shard_map/all_gather | solution.py:22
  204.1 1.6 fusion.3
  205.8 40.8 %all-gather.25.cloned.1.call-done = bf16[1,2048,256]{2,1,0:T(8,128)(2,1)} async-done(((bf16[1,256,256]{2,1,0:T(8,128)(2,1)}), bf16[1,2048,256]{2,1,0:T(8,128)(2,1)}) %all-gather.25.cloned.1.call-update) | async-done | bytes 1048592 | tf_op jit(solution)/shard_map/all_gather | solution.py:29
  246.6 2.0 fusion.19
  248.6 39.1 %all-gather.27.cloned.1.call-done = bf16[1,2048,256]{2,1,0:T(8,128)(2,1)} async-done(((bf16[1,256,256]{2,1,0:T(8,128)(2,1)}), bf16[1,2048,256]{2,1,0:T(8,128)(2,1)}) %all-gather.27.cloned.1.call-update) | async-done | bytes 1048592 | tf_op jit(solution)/shard_map/all_gather | solution.py:30
  287.7 0.0 copy-done.2
  287.7 1.7 fusion.15
  289.5 2.5 collective-permute-start.1
  292.0 1.9 collective-permute-done.1
  293.9 4.8 %fusion.51 = (f32[256]{0:T(256)S(1)}, f32[1,256,256]{2,0,1:T(1,128)S(1)}) fusion(f32[1,128,256]{2,1,0:T(8,128)S(1)} %get-tuple-element.5, bf16[1,383,256]{2,1,0:T(8,128)(2,1)S(1)} %maximum_bitcast_fusion.1), kind=kOutput, calls=%fused_computation.71 | convolution fusion | flops 100728576 | bytes 590336 | tf_op jit(solution)/shard_map/conv_general_dilated | solution.py:37
  298.8 5.7 %psum.30 = f32[256,1]{0,1:T(1,128)S(1)} all-reduce(f32[256,1]{0,1:T(1,128)S(1)} %bitcast.73), channel_id=1, replica_groups=mesh['sp'=8,'tp'=4] {'tp'}, use_global_device_ids=true, to_apply=%region_8.9 | all-reduce | flops 256 | bytes 2048 | tf_op jit(solution)/shard_map/psum | solution.py:46
  304.4 0.2 multiply_reduce_fusion
  304.6 7.0 %psum.31 = f32[256,1]{0,1:T(1,128)S(1)} all-reduce(f32[256,1]{0,1:T(1,128)S(1)} %bitcast.69), channel_id=1, replica_groups=mesh['sp'=8,'tp'=4] {'tp'}, use_global_device_ids=true, to_apply=%region_10.11 | all-reduce | flops 256 | bytes 2048 | tf_op jit(solution)/shard_map/psum | solution.py:48
  311.6 16.3 %all-gather.29.cloned.1.call-done = bf16[1,256,2048]{2,1,0:T(8,128)(2,1)} async-done(((bf16[1,256,256]{2,1,0:T(8,128)(2,1)}), bf16[1,256,2048]{2,1,0:T(8,128)(2,1)}) %all-gather.29.cloned.1.call-update) | async-done | bytes 1048592 | tf_op jit(solution)/shard_map/all_gather | solution.py:52
  327.9 3.1 fusion.16
  331.0 0.0 reduce-scatter.5.cloned.1.call-update
  331.1 30.3 %reduce-scatter.5.cloned.1.call-done = f32[256,512]{1,0:T(8,128)} async-done(((f32[256,2048]{1,0:T(8,128)}), f32[256,512]{1,0:T(8,128)}) %reduce-scatter.5.cloned.1.call-update) | async-done | bytes 524304 | tf_op jit(solution)/shard_map/reduce_scatter | solution.py:54
  361.4 0.0 copy-done
  361.4 1.8 add_convert_fusion
  (20 shorter events, 0.2 us)
Async XLA Ops:
  6.5 6.1 %copy-start.5 = (f32[2,2048]{1,0:T(2,128)S(1)}, f32[2,2048]{1,0:T(2,128)}, u32[]{:S(2)}) copy-start(f32[2,2048]{1,0:T(2,128)} %param.8) | copy-start | bytes 49156
  6.5 6.1 %copy-start.4 = (f32[2,128,256]{2,1,0:T(8,128)S(1)}, f32[2,128,256]{2,1,0:T(8,128)}, u32[]{:S(2)}) copy-start(f32[2,128,256]{2,1,0:T(8,128)} %param.11) | copy-start | bytes 786436
  6.5 21.8 %all-gather.15.cloned.1.call-start = ((), (), s32[]{:S(2)}) async-start(), calls=%async_computation.2 | async-start | bytes 1310720 | tf_op jit(solution)/shard_map/all_gather | solution.py:22
  7.3 63.5 %all-gather.19.cloned.1.call-start = ((), (), s32[]{:S(2)}) async-start(), calls=%async_computation.6 | async-start | bytes 1179648 | tf_op jit(solution)/shard_map/all_gather | solution.py:29
  9.0 102.9 %all-gather.21.cloned.1.call-start = ((), (), s32[]{:S(2)}) async-start(), calls=%async_computation.7 | async-start | bytes 1179648 | tf_op jit(solution)/shard_map/all_gather | solution.py:30
  10.8 141.2 %all-gather.23.cloned.1.call-start = ((), (), s32[]{:S(2)}) async-start(), calls=%async_computation.8 | async-start | bytes 1179648 | tf_op jit(solution)/shard_map/all_gather | solution.py:52
  12.6 172.9 %reduce-scatter.3.cloned.1.call-start = ((), (), s32[]{:S(2)}) async-start(), calls=%async_computation.3 | async-start | bytes 2621440 | tf_op jit(solution)/shard_map/reduce_scatter | solution.py:54
  28.4 83.6 %copy-start.1 = (bf16[256,2048]{1,0:T(8,128)(2,1)S(1)}, bf16[256,2048]{1,0:T(8,128)(2,1)}, u32[]{:S(2)}) copy-start(bf16[256,2048]{1,0:T(8,128)(2,1)} %all-gather.15.cloned.1.call-done) | copy-start | bytes 3145732
  72.8 43.4 %copy-start.6 = (f32[2,256]{1,0:T(2,128)S(1)}, f32[2,256]{1,0:T(2,128)}, u32[]{:S(2)}) copy-start(f32[2,256]{1,0:T(2,128)} %param.12) | copy-start | bytes 6148
  113.7 4.4 %collective-permute-start = (bf16[128,256]{1,0:T(8,128)(2,1)S(1)}, bf16[128,256]{1,0:T(8,128)(2,1)S(1)}, u32[]{:S(2)}, u32[]{:S(2)}) collective-permute-start(bf16[128,256]{1,0:T(8,128)(2,1)S(1)} %slice.64), channel_id=1, source_target_pairs={{0,4},{4,8},{8,12},{12,16},{16,20},{20,24},{24,28},{1,5},{5,9},{9,... | collective-permute-start | bytes 196616 | tf_op jit(solution)/shard_map/ppermute | solution.py:13
  152.0 33.5 %copy-start.3 = (bf16[256,512]{1,0:T(8,128)(2,1)S(1)}, bf16[256,512]{1,0:T(8,128)(2,1)}, u32[]{:S(2)}) copy-start(bf16[256,512]{1,0:T(8,128)(2,1)} %param.7) | copy-start | bytes 786436
  155.1 49.0 %all-gather.17.cloned.1.call-start = ((), (), s32[]{:S(2)}) async-start(), calls=%async_computation.4 | async-start | bytes 1310720 | tf_op jit(solution)/shard_map/all_gather | solution.py:22
  187.3 59.3 %all-gather.25.cloned.1.call-start = ((), (), s32[]{:S(2)}) async-start(), calls=%async_computation.9 | async-start | bytes 1179648 | tf_op jit(solution)/shard_map/all_gather | solution.py:29
  188.0 99.7 %all-gather.27.cloned.1.call-start = ((), (), s32[]{:S(2)}) async-start(), calls=%async_computation.10 | async-start | bytes 1179648 | tf_op jit(solution)/shard_map/all_gather | solution.py:30
  188.8 139.1 %all-gather.29.cloned.1.call-start = ((), (), s32[]{:S(2)}) async-start(), calls=%async_computation.11 | async-start | bytes 1179648 | tf_op jit(solution)/shard_map/all_gather | solution.py:52
  189.5 171.9 %reduce-scatter.5.cloned.1.call-start = ((), (), s32[]{:S(2)}) async-start(), calls=%async_computation.5 | async-start | bytes 2621440 | tf_op jit(solution)/shard_map/reduce_scatter | solution.py:54
  204.1 83.6 %copy-start.2 = (bf16[256,2048]{1,0:T(8,128)(2,1)S(1)}, bf16[256,2048]{1,0:T(8,128)(2,1)}, u32[]{:S(2)}) copy-start(bf16[256,2048]{1,0:T(8,128)(2,1)} %all-gather.17.cloned.1.call-done) | copy-start | bytes 3145732
  289.5 4.4 %collective-permute-start.1 = (bf16[128,256]{1,0:T(8,128)(2,1)S(1)}, bf16[128,256]{1,0:T(8,128)(2,1)S(1)}, u32[]{:S(2)}, u32[]{:S(2)}) collective-permute-start(bf16[128,256]{1,0:T(8,128)(2,1)S(1)} %slice.66), channel_id=1, source_target_pairs={{0,4},{4,8},{8,12},{12,16},{16,20},{20,24},{24,28},{1,5},{5,9},{9,... | collective-permute-start | bytes 196616 | tf_op jit(solution)/shard_map/ppermute | solution.py:13
  327.9 33.5 %copy-start = (bf16[256,512]{1,0:T(8,128)(2,1)S(1)}, bf16[256,512]{1,0:T(8,128)(2,1)}, u32[]{:S(2)}) copy-start(bf16[256,512]{1,0:T(8,128)(2,1)} %add_convert_fusion.1) | copy-start | bytes 786436
Sparse Core Ops, SparseCore 0:
  8.9 19.4 all-gather.14
  30.5 40.2 all-gather.18
  72.9 38.9 all-gather.20
  113.8 38.0 all-gather.22
  155.2 30.1 reduce-scatter.2
  187.4 16.6 all-gather.16
  206.3 40.2 all-gather.24
  248.7 38.9 all-gather.26
  289.8 38.0 all-gather.28
  331.2 30.1 reduce-scatter.4
where the time goes:
time: 371 us; the launch traced here: 370 us
  waiting for transfers between devices  290 us (78%)
  blocking collectives  25.3 us (7%)
  matrix products  23.4 us (6%)
  between operations  13.7 us (4%)
  other arithmetic  7.31 us (2%)
  starting transfers between devices  5.32 us (1%)
  local copies, waits for them, and re-layouts  5.19 us (1%)
    all_gather x2, waiting for transfers between devices, shards(): lax.all_gather(w_value[layer], 'sp', axis=0, tiled=True)  81.7 us
    all_gather x2, waiting for transfers between devices, shards(): lax.all_gather(w_gate[layer], 'sp', axis=0, tiled=True)  78.2 us
    reduce_scatter x2, waiting for transfers between devices, shards(): branch = lax.psum_scatter(terms, 'tp', scatter_dimension=1, tiled=True)  60.6 us
    all_gather x2, waiting for transfers between devices, shards(): out_whole = lax.all_gather(w_out[layer], 'sp', axis=1, tiled=True)  32.5 us
    all_gather x2, waiting for transfers between devices, shards(): whole = lax.all_gather(x, 'tp', axis=1, tiled=True).astype(jnp.float32)  30.3 us
    psum x2, blocking collectives, shards(): lax.psum(jnp.sum(centred * centred, axis=1, keepdims=True), 'tp') / C  14 us
    psum x2, blocking collectives, shards(): mean = lax.psum(jnp.sum(conv, axis=1, keepdims=True), 'tp') / C  11.3 us
    conv_general_dilated x2, matrix products, shards(): lax.conv_general_dilated(padded[None], conv_taps[layer][:, None, :], (1,)...  9.67 us
  transfers between devices with their start and end apart: 12, of which 12 were waited for; matrix products, arithmetic and copies ran while one was open for 7% of the time, Pallas kernels for 0%

commit v1 on v0

--- a/solution.py
+++ b/solution.py
@@ -49,7 +49,9 @@
         act = jax.nn.silu(centred * lax.rsqrt(spread + 1e-05) * channel_gain[layer]).astype(
             jnp.bfloat16
         )
-        out_whole = lax.all_gather(w_out[layer], "sp", axis=1, tiled=True)
+        block = w_out[layer]
+        blocks = lax.all_gather(block, "sp")
+        out_whole = jnp.concatenate(blocks, axis=1)
         terms = jnp.dot(act, out_whole, preferred_element_type=jnp.float32)
         branch = lax.psum_scatter(terms, "tp", scatter_dimension=1, tiled=True)
         x = (x.astype(jnp.float32) + branch).astype(jnp.bfloat16)

time: 371 us -> 406 us (1.094)
  waiting for transfers between devices: 290 us -> 326 us
    all_gather x2, waiting for transfers between devices: 32.5 us -> 73.6 us  [shards(): blocks = lax.all_gather(block, 'sp')]
  transfers between devices with their start and end apart: 12 -> 12, of which waited for: 12 -> 10; matrix products, arithmetic and copies ran while one was open for 7% -> 5% of each run, Pallas kernels for 0% -> 0%
where the time goes in v1:
time: 406 us; the launch traced here: 405 us
  waiting for transfers between devices  326 us (80%)
  blocking collectives  24.5 us (6%)
  matrix products  20.9 us (5%)
  between operations  13.7 us (3%)
  local copies, waits for them, and re-layouts  8.14 us (2%)
  other arithmetic  7.31 us (2%)
  starting transfers between devices  5.32 us (1%)
    all_gather x2, waiting for transfers between devices, shards(): lax.all_gather(w_value[layer], 'sp', axis=0, tiled=True)  81.7 us
    all_gather x2, waiting for transfers between devices, shards(): lax.all_gather(w_gate[layer], 'sp', axis=0, tiled=True)  78.2 us
    all_gather x2, waiting for transfers between devices, shards(): blocks = lax.all_gather(block, 'sp')  73.6 us
    reduce_scatter x2, waiting for transfers between devices, shards(): branch = lax.psum_scatter(terms, 'tp', scatter_dimension=1, tiled=True)  58.9 us
    all_gather x2, waiting for transfers between devices, shards(): whole = lax.all_gather(x, 'tp', axis=1, tiled=True).astype(jnp.float32)  30.2 us
    psum x2, blocking collectives, shards(): lax.psum(jnp.sum(centred * centred, axis=1, keepdims=True), 'tp') / C  13.2 us
    psum x2, blocking collectives, shards(): mean = lax.psum(jnp.sum(conv, axis=1, keepdims=True), 'tp') / C  11.3 us
    conv_general_dilated x2, matrix products, shards(): lax.conv_general_dilated(padded[None], conv_taps[layer][:, None, :], (1,)...  9.67 us
  transfers between devices with their start and end apart: 12, of which 10 were waited for; matrix products, arithmetic and copies ran while one was open for 5% of the time, Pallas kernels for 0%

profile of v1, /device:TPU:0, one launch (start us, length us, event | category | flops | bytes accessed | tf_op | source)
XLA Modules:
  0.0 405.4 jit_solution(7602448940463626116)
XLA Ops:
  6.5 0.0 all-gather.13.cloned.1.call-start
  6.5 0.7 all-gather.13.cloned.1.call-update
  7.3 0.0 all-gather.21.cloned.1.call-start
  7.3 1.7 fusion.48
  9.0 0.0 all-gather.21.cloned.1.call-update
  9.0 0.0 all-gather.23.cloned.1.call-start
  9.1 1.7 fusion.47
  10.8 0.0 all-gather.23.cloned.1.call-update
  10.8 0.0 all-gather.15.cloned.1.call-start
  10.8 1.7 fusion.49
  12.5 0.0 all-gather.15.cloned.1.call-update
  12.6 0.0 reduce-scatter.3.cloned.1.call-start
  12.6 0.0 copy-done.4
  12.6 0.0 copy-done.5
  12.7 15.7 %all-gather.13.cloned.1.call-done = bf16[256,2048]{1,0:T(8,128)(2,1)} async-done(((bf16[256,512]{1,0:T(8,128)(2,1)}), bf16[256,2048]{1,0:T(8,128)(2,1)}) %all-gather.13.cloned.1.call-update) | async-done | bytes 1048592 | tf_op jit(solution)/shard_map/all_gather | solution.py:22
  28.4 1.6 fusion
  30.0 40.8 %all-gather.21.cloned.1.call-done = bf16[1,2048,256]{2,1,0:T(8,128)(2,1)} async-done(((bf16[1,256,256]{2,1,0:T(8,128)(2,1)}), bf16[1,2048,256]{2,1,0:T(8,128)(2,1)}) %all-gather.21.cloned.1.call-update) | async-done | bytes 1048592 | tf_op jit(solution)/shard_map/all_gather | solution.py:29
  70.8 2.0 fusion.20
  72.8 0.0 copy-start.6
  72.8 39.1 %all-gather.23.cloned.1.call-done = bf16[1,2048,256]{2,1,0:T(8,128)(2,1)} async-done(((bf16[1,256,256]{2,1,0:T(8,128)(2,1)}), bf16[1,2048,256]{2,1,0:T(8,128)(2,1)}) %all-gather.23.cloned.1.call-update) | async-done | bytes 1048592 | tf_op jit(solution)/shard_map/all_gather | solution.py:30
  111.9 0.0 copy-done.1
  111.9 1.7 fusion.14
  113.7 2.5 collective-permute-start
  116.2 0.0 copy-done.6
  116.2 36.7 %all-gather.15.cloned.1.call-done = bf16[8,256,256]{2,1,0:T(8,128)(2,1)} async-done(((bf16[1,256,256]{2,1,0:T(8,128)(2,1)}), bf16[8,256,256]{2,1,0:T(8,128)(2,1)}) %all-gather.15.cloned.1.call-update) | async-done | bytes 1048592 | tf_op jit(solution)/shard_map/all_gather | solution.py:53
  152.9 1.5 copy.27
  154.4 0.0 collective-permute-done
  154.5 4.8 %fusion.52 = (f32[256]{0:T(256)S(1)}, f32[1,256,256]{2,0,1:T(1,128)S(1)}) fusion(f32[1,128,256]{2,1,0:T(8,128)S(1)} %get-tuple-element.6, bf16[1,383,256]{2,1,0:T(8,128)(2,1)S(1)} %maximum_bitcast_fusion), kind=kOutput, calls=%fused_computation.70 | convolution fusion | flops 100728576 | bytes 590336 | tf_op jit(solution)/shard_map/conv_general_dilated | solution.py:37
  159.3 5.7 %psum.28 = f32[256,1]{0,1:T(1,128)S(1)} all-reduce(f32[256,1]{0,1:T(1,128)S(1)} %bitcast.80), channel_id=1, replica_groups=mesh['sp'=8,'tp'=4] {'tp'}, use_global_device_ids=true, to_apply=%region_2.0 | all-reduce | flops 256 | bytes 2048 | tf_op jit(solution)/shard_map/psum | solution.py:46
  165.0 0.2 fusion.33
  165.2 6.6 %psum.29 = f32[256,1]{0,1:T(1,128)S(1)} all-reduce(f32[256,1]{0,1:T(1,128)S(1)} %bitcast.76), channel_id=1, replica_groups=mesh['sp'=8,'tp'=4] {'tp'}, use_global_device_ids=true, to_apply=%region_4.0 | all-reduce | flops 256 | bytes 2048 | tf_op jit(solution)/shard_map/psum | solution.py:48
  171.8 1.8 fusion.36
  173.7 0.0 reduce-scatter.3.cloned.1.call-update
  173.7 0.0 all-gather.17.cloned.1.call-start
  173.7 29.4 %reduce-scatter.3.cloned.1.call-done = f32[256,512]{1,0:T(8,128)} async-done(((f32[256,2048]{1,0:T(8,128)}), f32[256,512]{1,0:T(8,128)}) %reduce-scatter.3.cloned.1.call-update) | async-done | bytes 524304 | tf_op jit(solution)/shard_map/reduce_scatter | solution.py:56
  203.1 0.0 copy-done.3
  203.1 1.8 add_convert_fusion.1
  204.9 0.0 all-gather.17.cloned.1.call-update
  205.0 0.0 all-gather.25.cloned.1.call-start
  205.0 0.7 all-gather.25.cloned.1.call-update
  205.7 0.0 all-gather.27.cloned.1.call-start
  205.8 0.7 all-gather.27.cloned.1.call-update
  206.5 0.0 all-gather.19.cloned.1.call-start
  206.5 0.7 all-gather.19.cloned.1.call-update
  207.2 0.0 reduce-scatter.5.cloned.1.call-start
  207.3 14.6 %all-gather.17.cloned.1.call-done = bf16[256,2048]{1,0:T(8,128)(2,1)} async-done(((bf16[256,512]{1,0:T(8,128)(2,1)}), bf16[256,2048]{1,0:T(8,128)(2,1)}) %all-gather.17.cloned.1.call-update) | async-done | bytes 1048592 | tf_op jit(solution)/shard_map/all_gather | solution.py:22
  221.8 1.6 fusion.3
  223.4 40.8 %all-gather.25.cloned.1.call-done = bf16[1,2048,256]{2,1,0:T(8,128)(2,1)} async-done(((bf16[1,256,256]{2,1,0:T(8,128)(2,1)}), bf16[1,2048,256]{2,1,0:T(8,128)(2,1)}) %all-gather.25.cloned.1.call-update) | async-done | bytes 1048592 | tf_op jit(solution)/shard_map/all_gather | solution.py:29
  264.3 2.0 fusion.17
  266.3 39.1 %all-gather.27.cloned.1.call-done = bf16[1,2048,256]{2,1,0:T(8,128)(2,1)} async-done(((bf16[1,256,256]{2,1,0:T(8,128)(2,1)}), bf16[1,2048,256]{2,1,0:T(8,128)(2,1)}) %all-gather.27.cloned.1.call-update) | async-done | bytes 1048592 | tf_op jit(solution)/shard_map/all_gather | solution.py:30
  305.4 1.7 fusion.15
  307.2 2.5 collective-permute-start.1
  309.6 36.9 %all-gather.19.cloned.1.call-done = bf16[8,256,256]{2,1,0:T(8,128)(2,1)} async-done(((bf16[1,256,256]{2,1,0:T(8,128)(2,1)}), bf16[8,256,256]{2,1,0:T(8,128)(2,1)}) %all-gather.19.cloned.1.call-update) | async-done | bytes 1048592 | tf_op jit(solution)/shard_map/all_gather | solution.py:53
  346.6 1.5 copy.31
  348.0 0.0 collective-permute-done.1
  348.1 4.8 %fusion.53 = (f32[256]{0:T(256)S(1)}, f32[1,256,256]{2,0,1:T(1,128)S(1)}) fusion(f32[1,128,256]{2,1,0:T(8,128)S(1)} %get-tuple-element.5, bf16[1,383,256]{2,1,0:T(8,128)(2,1)S(1)} %maximum_bitcast_fusion.1), kind=kOutput, calls=%fused_computation.71 | convolution fusion | flops 100728576 | bytes 590336 | tf_op jit(solution)/shard_map/conv_general_dilated | solution.py:37
  353.0 5.7 %psum.30 = f32[256,1]{0,1:T(1,128)S(1)} all-reduce(f32[256,1]{0,1:T(1,128)S(1)} %bitcast.81), channel_id=1, replica_groups=mesh['sp'=8,'tp'=4] {'tp'}, use_global_device_ids=true, to_apply=%region_8.9 | all-reduce | flops 256 | bytes 2048 | tf_op jit(solution)/shard_map/psum | solution.py:46
  358.6 0.2 fusion.31
  358.8 6.6 %psum.31 = f32[256,1]{0,1:T(1,128)S(1)} all-reduce(f32[256,1]{0,1:T(1,128)S(1)} %bitcast.77), channel_id=1, replica_groups=mesh['sp'=8,'tp'=4] {'tp'}, use_global_device_ids=true, to_apply=%region_10.11 | all-reduce | flops 256 | bytes 2048 | tf_op jit(solution)/shard_map/psum | solution.py:48
  365.4 1.8 fusion.34
  367.3 0.0 reduce-scatter.5.cloned.1.call-update
  367.3 29.5 %reduce-scatter.5.cloned.1.call-done = f32[256,512]{1,0:T(8,128)} async-done(((f32[256,2048]{1,0:T(8,128)}), f32[256,512]{1,0:T(8,128)}) %reduce-scatter.5.cloned.1.call-update) | async-done | bytes 524304 | tf_op jit(solution)/shard_map/reduce_scatter | solution.py:56
  396.8 0.0 copy-done
  396.8 1.8 add_convert_fusion
  (22 shorter events, 0.2 us)
Async XLA Ops:
  6.5 6.1 %copy-start.4 = (f32[2,128,256]{2,1,0:T(8,128)S(1)}, f32[2,128,256]{2,1,0:T(8,128)}, u32[]{:S(2)}) copy-start(f32[2,128,256]{2,1,0:T(8,128)} %param.11) | copy-start | bytes 786436
  6.5 6.1 %copy-start.5 = (f32[2,2048]{1,0:T(2,128)S(1)}, f32[2,2048]{1,0:T(2,128)}, u32[]{:S(2)}) copy-start(f32[2,2048]{1,0:T(2,128)} %param.8) | copy-start | bytes 49156
  6.5 21.8 %all-gather.13.cloned.1.call-start = ((), (), s32[]{:S(2)}) async-start(), calls=%async_computation.2 | async-start | bytes 1310720 | tf_op jit(solution)/shard_map/all_gather | solution.py:22
  7.3 63.5 %all-gather.21.cloned.1.call-start = ((), (), s32[]{:S(2)}) async-start(), calls=%async_computation.8 | async-start | bytes 1179648 | tf_op jit(solution)/shard_map/all_gather | solution.py:29
  9.0 102.9 %all-gather.23.cloned.1.call-start = ((), (), s32[]{:S(2)}) async-start(), calls=%async_computation.9 | async-start | bytes 1179648 | tf_op jit(solution)/shard_map/all_gather | solution.py:30
  10.8 142.1 %all-gather.15.cloned.1.call-start = ((), (), s32[]{:S(2)}) async-start(), calls=%async_computation.3 | async-start | bytes 1179648 | tf_op jit(solution)/shard_map/all_gather | solution.py:53
  12.6 190.6 %reduce-scatter.3.cloned.1.call-start = ((), (), s32[]{:S(2)}) async-start(), calls=%async_computation.4 | async-start | bytes 2621440 | tf_op jit(solution)/shard_map/reduce_scatter | solution.py:56
  28.4 83.6 %copy-start.1 = (bf16[256,2048]{1,0:T(8,128)(2,1)S(1)}, bf16[256,2048]{1,0:T(8,128)(2,1)}, u32[]{:S(2)}) copy-start(bf16[256,2048]{1,0:T(8,128)(2,1)} %all-gather.13.cloned.1.call-done) | copy-start | bytes 3145732
  72.8 43.4 %copy-start.6 = (f32[2,256]{1,0:T(2,128)S(1)}, f32[2,256]{1,0:T(2,128)}, u32[]{:S(2)}) copy-start(f32[2,256]{1,0:T(2,128)} %param.12) | copy-start | bytes 6148
  113.7 40.7 %collective-permute-start = (bf16[128,256]{1,0:T(8,128)(2,1)S(1)}, bf16[128,256]{1,0:T(8,128)(2,1)S(1)}, u32[]{:S(2)}, u32[]{:S(2)}) collective-permute-start(bf16[128,256]{1,0:T(8,128)(2,1)S(1)} %slice.64), channel_id=1, source_target_pairs={{0,4},{4,8},{8,12},{12,16},{16,20},{20,24},{24,28},{1,5},{5,9},{9,... | collective-permute-start | bytes 196616 | tf_op jit(solution)/shard_map/ppermute | solution.py:13
  171.8 31.3 %copy-start.3 = (bf16[256,512]{1,0:T(8,128)(2,1)S(1)}, bf16[256,512]{1,0:T(8,128)(2,1)}, u32[]{:S(2)}) copy-start(bf16[256,512]{1,0:T(8,128)(2,1)} %param.7) | copy-start | bytes 786436
  173.7 48.1 %all-gather.17.cloned.1.call-start = ((), (), s32[]{:S(2)}) async-start(), calls=%async_computation.5 | async-start | bytes 1310720 | tf_op jit(solution)/shard_map/all_gather | solution.py:22
  205.0 59.3 %all-gather.25.cloned.1.call-start = ((), (), s32[]{:S(2)}) async-start(), calls=%async_computation.10 | async-start | bytes 1179648 | tf_op jit(solution)/shard_map/all_gather | solution.py:29
  205.7 99.7 %all-gather.27.cloned.1.call-start = ((), (), s32[]{:S(2)}) async-start(), calls=%async_computation.11 | async-start | bytes 1179648 | tf_op jit(solution)/shard_map/all_gather | solution.py:30
  206.5 140.1 %all-gather.19.cloned.1.call-start = ((), (), s32[]{:S(2)}) async-start(), calls=%async_computation.6 | async-start | bytes 1179648 | tf_op jit(solution)/shard_map/all_gather | solution.py:53
  207.2 189.6 %reduce-scatter.5.cloned.1.call-start = ((), (), s32[]{:S(2)}) async-start(), calls=%async_computation.7 | async-start | bytes 2621440 | tf_op jit(solution)/shard_map/reduce_scatter | solution.py:56
  221.8 83.6 %copy-start.2 = (bf16[256,2048]{1,0:T(8,128)(2,1)S(1)}, bf16[256,2048]{1,0:T(8,128)(2,1)}, u32[]{:S(2)}) copy-start(bf16[256,2048]{1,0:T(8,128)(2,1)} %all-gather.17.cloned.1.call-done) | copy-start | bytes 3145732
  307.2 40.9 %collective-permute-start.1 = (bf16[128,256]{1,0:T(8,128)(2,1)S(1)}, bf16[128,256]{1,0:T(8,128)(2,1)S(1)}, u32[]{:S(2)}, u32[]{:S(2)}) collective-permute-start(bf16[128,256]{1,0:T(8,128)(2,1)S(1)} %slice.66), channel_id=1, source_target_pairs={{0,4},{4,8},{8,12},{12,16},{16,20},{20,24},{24,28},{1,5},{5,9},{9,... | collective-permute-start | bytes 196616 | tf_op jit(solution)/shard_map/ppermute | solution.py:13
  365.4 31.4 %copy-start = (bf16[256,512]{1,0:T(8,128)(2,1)S(1)}, bf16[256,512]{1,0:T(8,128)(2,1)}, u32[]{:S(2)}) copy-start(bf16[256,512]{1,0:T(8,128)(2,1)} %add_convert_fusion.1) | copy-start | bytes 786436
Sparse Core Ops, SparseCore 0:
  8.9 19.4 all-gather.12
  30.5 40.2 all-gather.20
  72.9 38.9 all-gather.22
  113.9 38.9 all-gather.14
  173.8 29.2 reduce-scatter.2
  205.1 16.6 all-gather.16
  223.9 40.2 all-gather.24
  266.4 38.9 all-gather.26
  307.5 38.9 all-gather.18
  367.4 29.3 reduce-scatter.4
